TPU v7x, 256 devices: a whole 4x4x8 slice. The times are simulated.
256 devices in a mesh: sp: 32 (over z, x), tp: 8 (over y, core).
Axes of the slice: x: 4, y: 4, z: 8, core: 2. Of those that a mesh axis runs over, the one named last changes fastest.
Arguments:
- residual: bfloat16 [24576, 2048], P('sp'), may hold values from -6 to 6
- queries: bfloat16 [24576, 1024], P('sp', 'tp'), may hold values from -12 to 12
- keys: bfloat16 [24576, 512], P('sp', 'tp'), may hold values from -6 to 6
- values: bfloat16 [24576, 512], P('sp', 'tp'), may hold values from -36 to 36
- segments: int32 [24576], P('sp'), may hold values from 0 to 15, never falling along the last dimension, each value on 1 to 3072 neighbouring positions
- sink: float32 [16], P('tp'), may hold values from 3 to 7
- out_weight: bfloat16 [1024, 2048], replicated, may hold values from -0.1875 to 0.1875
- norm_gain_one: float32 [2048], replicated, may hold values from 0.1 to 1.9
- group: int32 [24576], P('sp'), may hold values from 0 to 3, as said below
- member: int32 [24576, 2], P('sp'), may hold values from 0 to 7, as said below
- route_weight: float32 [24576, 2], P('sp'), may hold values from 0.25 to 1
- gate_weight: bfloat16 [32, 2048, 1024], P('sp', None, 'tp'), may hold values from -0.125 to 0.125
- up_weight: bfloat16 [32, 2048, 1024], P('sp', None, 'tp'), may hold values from -0.125 to 0.125
- down_weight: bfloat16 [32, 1024, 2048], P('sp', None, 'tp'), may hold values from -0.1875 to 0.1875
- norm_gain_two: float32 [2048], P('tp'), may hold values from 0.1 to 1.9
Outputs:
- output: bfloat16 [24576, 2048], P('sp', 'tp')
Inputs may be any that keep to these rules, and one draw needn't show every extreme that they name: In every aligned block of 96 rows no expert (group * 8 + member) is named by more than 12 rows, and one expert, the same in all blocks of a draw, is named by exactly 12 rows of every block. `member`: the 2 members of a row differ.
All inputs are finite; a program needn't handle non-finite values.
Results may differ from a plain program's by a relative error of at most 0.0059.
Values may be sent and summed in bfloat16 or wider, within the bound.
No kernel may reach another device: no remote copies, remote signals or barrier semaphores. Data moves between devices by JAX's collectives and lax.ppermute only.
A program may use at most 128 MiB of HBM per device.

v0:
```python
import math
import jax
import jax.numpy as jnp
from jax import lax
from jax.sharding import PartitionSpec as P

HEAD_DIM = 64
HALF = 128
PER_GROUP = 8
ALPHA = 2.0**0.25
EPS = 1e-05


def with_halo(block, sides, width):
    for axis, dim in sides:
        count = lax.axis_size(axis)
        forward = [(i, i + 1) for i in range(count - 1)]
        backward = [(target, source) for source, target in forward]
        low = lax.ppermute(
            lax.slice_in_dim(block, block.shape[dim] - width, None, axis=dim), axis, forward
        )
        high = lax.ppermute(lax.slice_in_dim(block, 0, width, axis=dim), axis, backward)
        block = jnp.concatenate([low, block, high], axis=dim)
    return block


def copy_for_each(x, axis):
    copies = jnp.broadcast_to(x, (lax.axis_size(axis), *x.shape))
    return lax.all_to_all(copies, axis, split_axis=0, concat_axis=0, tiled=True)


def joined_along(pieces, dim):
    pieces = jnp.moveaxis(pieces, 0, dim)
    lengths = pieces.shape
    return pieces.reshape(*lengths[:dim], lengths[dim] * lengths[dim + 1], *lengths[dim + 2 :])


def gather_directly(x, axis, dim):
    pieces = copy_for_each(x, axis)
    return joined_along(pieces, dim)


def taken_together(x, axis):
    everything = copy_for_each(x, axis)
    return jnp.sum(everything, axis=0)


def packed_total(arrays, axis):
    ends = [0]
    for a in arrays:
        ends.append(ends[-1] + a.size)
    subtotal = taken_together(jnp.concatenate([a.ravel() for a in arrays]), axis)
    return tuple((subtotal[b:e].reshape(a.shape) for a, b, e in zip(arrays, ends, ends[1:])))


def layer_norm(summed, norm_gain):
    mean_value = jnp.mean(summed, -1, keepdims=True)
    variance = jnp.mean(jnp.square(summed - mean_value), -1, keepdims=True)
    return ((summed - mean_value) * lax.rsqrt(variance + EPS) * norm_gain).astype(jnp.bfloat16)


def shards(
    residual,
    queries,
    keys,
    values,
    segments,
    sink,
    out_weight,
    norm_gain_one,
    group,
    member,
    route_weight,
    gate_weight,
    up_weight,
    down_weight,
    norm_gain_two,
):
    row_count = queries.shape[0]
    sp_size = lax.axis_size("sp")
    tp_size = lax.axis_size("tp")
    kv_local = keys.shape[1] // HEAD_DIM
    heads_local = queries.shape[1] // HEAD_DIM
    group_size = heads_local // kv_local
    seq_total = row_count * sp_size
    seq_start = lax.axis_index("sp") * row_count
    joined = jnp.concatenate([keys, values], axis=1)
    padded, seg_padded = (
        with_halo(joined, (("sp", 0),), HALF),
        with_halo(segments, (("sp", 0),), HALF),
    )
    query_block = math.gcd(row_count, 512)
    key_span = query_block + 2 * HALF
    offsets = jnp.arange(key_span)[None, :] - HALF - jnp.arange(query_block)[:, None]
    in_band = jnp.abs(offsets) <= HALF
    sink_heads = sink.reshape(kv_local, group_size, 1, 1)
    query_heads = queries.reshape(row_count, kv_local, group_size, HEAD_DIM)
    key_cols = kv_local * HEAD_DIM
    pieces = []
    for number in range(row_count // query_block):
        row_low = number * query_block
        query_rows = query_heads[row_low : row_low + query_block]
        kv_rows = padded[row_low : row_low + key_span]
        key_part = kv_rows[:, :key_cols].reshape(key_span, kv_local, HEAD_DIM)
        value_part = kv_rows[:, key_cols:].reshape(key_span, kv_local, HEAD_DIM)
        key_place = seq_start + row_low - HALF + jnp.arange(key_span)
        inside = (key_place >= 0) & (key_place < seq_total)
        same_doc = (
            segments[row_low : row_low + query_block, None]
            == seg_padded[None, row_low : row_low + key_span]
        )
        allowed = in_band & same_doc & inside[None, :]
        scores = jnp.einsum(
            "qkgd,ckd->kgqc", query_rows, key_part, preferred_element_type=jnp.float32
        ) * HEAD_DIM ** (-0.5)
        masked = jnp.where(allowed, scores, -1e30)
        peak = jnp.maximum(jnp.max(masked, -1, keepdims=True), sink_heads)
        raised = jnp.where(allowed, jnp.exp(masked - peak), 0.0)
        denominator = jnp.sum(raised, -1, keepdims=True) + jnp.exp(sink_heads - peak)
        weights = (raised / denominator).astype(jnp.bfloat16)
        attended_part = jnp.einsum(
            "kgqc,ckd->qkgd", weights, value_part, preferred_element_type=jnp.float32
        )
        pieces.append(
            attended_part.reshape(query_block, heads_local * HEAD_DIM).astype(jnp.bfloat16)
        )
    attended = jnp.concatenate(pieces, 0)
    width = out_weight.shape[1]
    weight_rows = out_weight
    mixed = jnp.dot(
        gather_directly(attended, "tp", 1), weight_rows, preferred_element_type=jnp.float32
    )
    pre_one = ALPHA * residual.astype(jnp.float32) + mixed
    normed = layer_norm(pre_one, norm_gain_one)
    experts_local = gate_weight.shape[0]
    expert_count = experts_local * sp_size
    picks_count = member.shape[1]
    block_rows = row_count // tp_size
    capacity = max(2, block_rows // 8)
    expert_ids = (group[:, None] * PER_GROUP + member).reshape(tp_size, block_rows * picks_count)
    onehot_table = (expert_ids[:, :, None] == jnp.arange(expert_count)[None, None, :]).astype(
        jnp.int32
    )
    ranks = jnp.sum((jnp.cumsum(onehot_table, 1) - 1) * onehot_table, 2)
    owner = expert_ids // experts_local
    local_ids = expert_ids % experts_local
    block_ids = jnp.arange(tp_size)[:, None]
    slot_all = ((local_ids * sp_size + owner) * tp_size + block_ids) * capacity + ranks
    copy_rows = (
        jnp.arange(row_count * picks_count).reshape(tp_size, block_rows * picks_count)
        // picks_count
    )
    extended = jnp.concatenate([normed, jnp.zeros((1, width), jnp.bfloat16)], 0)
    tp_place = lax.axis_index("tp")
    slot_own_base = (local_ids * sp_size + owner) * capacity + ranks
    own_slots = lax.dynamic_index_in_dim(slot_own_base, tp_place, 0, keepdims=False)
    own_rows = lax.dynamic_index_in_dim(copy_rows, tp_place, 0, keepdims=False)
    slot_count = experts_local * sp_size * capacity
    source = jnp.full((slot_count,), row_count, jnp.int32).at[own_slots].set(own_rows)
    outgoing = extended[source].reshape(experts_local, sp_size, capacity, width)
    received = lax.all_to_all(outgoing, "sp", split_axis=1, concat_axis=1, tiled=True)
    arrived = lax.all_gather(received, "tp", axis=2, tiled=True)
    expert_rows = arrived.reshape(experts_local, sp_size * tp_size * capacity, width)
    gate_part = jnp.einsum(
        "esd,edf->esf", expert_rows, gate_weight, preferred_element_type=jnp.float32
    )
    up_part = jnp.einsum("esd,edf->esf", expert_rows, up_weight, preferred_element_type=jnp.float32)
    hidden = (jax.nn.silu(gate_part) * up_part).astype(jnp.bfloat16)
    column_width = down_weight.shape[2]
    weight_rows = down_weight
    produced = jnp.einsum(
        "esf,efc->esc",
        lax.all_gather(hidden, "tp", axis=2, tiled=True),
        weight_rows,
        preferred_element_type=jnp.float32,
    ).astype(jnp.bfloat16)
    returned = lax.all_to_all(
        produced.reshape(experts_local, sp_size, tp_size * capacity, column_width),
        "sp",
        split_axis=1,
        concat_axis=1,
        tiled=True,
    )
    result_rows = returned.reshape(-1, column_width)
    picked = result_rows[slot_all.reshape(row_count, picks_count)]
    combined = jnp.sum(route_weight[:, :, None] * picked.astype(jnp.float32), 1)
    column_start = lax.axis_index("tp") * column_width
    normed_part = lax.dynamic_slice_in_dim(normed, column_start, column_width, 1)
    pre_two = ALPHA * normed_part.astype(jnp.float32) + combined
    sums, squares = packed_total((jnp.sum(pre_two, -1), jnp.sum(pre_two * pre_two, -1)), "tp")
    mean_value = (sums / width)[:, None]
    variance = (squares / width)[:, None] - mean_value * mean_value
    return ((pre_two - mean_value) * lax.rsqrt(variance + EPS) * norm_gain_two).astype(jnp.bfloat16)


def solution(mesh):
    in_specs = (
        P("sp", None),
        P("sp", "tp"),
        P("sp", "tp"),
        P("sp", "tp"),
        P("sp"),
        P("tp"),
        P(),
        P(),
        P("sp"),
        P("sp", None),
        P("sp", None),
        P("sp", None, "tp"),
        P("sp", None, "tp"),
        P("sp", None, "tp"),
        P("tp"),
    )
    out_specs = P("sp", "tp")
    return jax.shard_map(shards, mesh=mesh, in_specs=in_specs, out_specs=out_specs, check_vma=False)
```

profile of v0, /device:TPU:1, one launch (start us, length us, event | category | flops | bytes accessed | tf_op | source)
XLA Modules:
  0.0 366.8 jit_solution(6680165087132534622)
XLA Ops:
  7.4 3.9 %collective-permute-start.1 = (s32[128]{0:T(128)S(1)}, s32[128]{0:T(128)S(1)}, u32[]{:S(2)}, u32[]{:S(2)}) collective-permute-start(s32[128]{0:T(128)S(1)} %get-tuple-element.16), channel_id=1, source_target_pairs={{0,8},{8,16},{16,24},{24,32},{32,40},{40,48},{48,56},{56,64},{64,7... | collective-permute-start | bytes 1544 | tf_op jit(solution)/shard_map/ppermute | solution.py:19
  11.3 1.3 collective-permute-start.3
  12.6 0.9 constant_dynamic-update-slice_fusion.1
  14.4 4.0 %collective-permute-start = (bf16[128,128]{0,1:T(8,128)(2,1)S(1)}, bf16[128,128]{0,1:T(8,128)(2,1)S(1)}, u32[]{:S(2)}, u32[]{:S(2)}) collective-permute-start(bf16[128,128]{0,1:T(8,128)(2,1)S(1)} %get-tuple-element.7), channel_id=1, source_target_pairs={{0,8},{8,16},{16,24},{24,32},{32,40},{40,48},{48,56},{56,64},{64,7... | collective-permute-start | bytes 98312 | tf_op jit(solution)/shard_map/ppermute | solution.py:19
  18.4 1.3 collective-permute-start.2
  21.2 0.9 fusion.63
  28.5 1.3 broadcast_in_dim.73
  29.7 6.0 %all-to-all-start = ((bf16[8,768,128]{1,2,0:T(8,128)(2,1)}), bf16[8,768,128]{1,2,0:T(8,128)(2,1)S(1)}, u32[]{:S(2)}, u32[]{:S(2)}) async-start(bf16[8,768,128]{1,2,0:T(8,128)(2,1)} %broadcast_in_dim.73), calls=%async_computation | async-start | bytes 3145728 | tf_op jit(solution)/shard_map/all_to_all | solution.py:29
  35.7 4.6 %reduce-window.6 = s32[8,32,2,128]{3,1,2,0:T(8,128)S(1)} reduce-window(s32[8,32,2,128]{3,1,2,0:T(8,128)S(1)} %copy_bitcast_fusion, s32[]{:T(128)} %constant.104.clone.1), window={size=1x1x1x128 pad=0_0x0_0x0_0x127_0}, to_apply=%region_8.9 | reduce-window | flops 8323072 | bytes 524292 | tf_op jit(solution)/shard_map/reduce-window
  41.0 1.4 scatter_custom_fusion
  42.4 13.9 %all-to-all-done = bf16[8,768,128]{1,2,0:T(8,128)(2,1)S(1)} async-done(((bf16[8,768,128]{1,2,0:T(8,128)(2,1)}), bf16[8,768,128]{1,2,0:T(8,128)(2,1)S(1)}, u32[]{:S(2)}, u32[]{:S(2)}) %all-to-all-start) | async-done | bytes 1572896 | tf_op jit(solution)/shard_map/all_to_all | solution.py:29
  56.3 7.3 %fusion.69 = (f32[768]{0:T(1024)S(1)}, f32[768,2048]{1,0:T(8,128)S(1)}) fusion(bf16[768,1024]{0,1:T(8,128)(2,1)S(1)} %bitcast.123, bf16[1024,2048]{1,0:T(8,128)(2,1)} %param.21, bf16[768,2048]{1,0:T(8,128)(2,1)} %param.15), kind=kOutput, calls=%fused_computation.143 | convolution fusion | flops 3227516160 | bytes 15207424 | tf_op jit(solution)/shard_map/dot_general | solution.py:130
  65.4 1.7 copy-done.1
  67.0 2.0 concatenate.32
  69.1 7.4 %gather_fusion = bf16[384,2048]{1,0:T(8,128)(2,1)} fusion(bf16[769,2048]{1,0:T(8,128)(2,1)} %concatenate.32, s32[1024]{0:T(1024)S(1)} %pad_clamp_fusion.1), kind=kCustom, calls=%fused_computation | custom fusion | bytes 3147264 | tf_op jit(solution)/shard_map/gather | solution.py:160
  76.4 2.4 reshape.420
  78.8 64.7 %all_to_all.21 = bf16[1,32,12,2048]{3,2,0,1:T(8,128)(2,1)S(1)} all-to-all(bf16[1,32,12,2048]{3,2,0,1:T(8,128)(2,1)S(1)} %bitcast.122), channel_id=1, replica_groups=mesh['sp'=32,'tp'=8] {'sp'}, dimensions={1} | all-to-all | bytes 3145728 | tf_op jit(solution)/shard_map/all_to_all | solution.py:161
  143.5 2.0 copy.96
  145.8 67.6 %all-gather.4.cloned.1.call-done = bf16[1,32,96,2048]{3,1,0,2:T(8,128)(2,1)} async-done(((bf16[1,32,12,2048]{3,1,0,2:T(8,128)(2,1)}), bf16[1,32,96,2048]{3,1,0,2:T(8,128)(2,1)}) %all-gather.4.cloned.1.call-update) | async-done | bytes 12582928 | tf_op jit(solution)/shard_map/all_gather | solution.py:162
  213.4 11.7 %copy.97 = bf16[1,32,96,2048]{3,2,1,0:T(8,128)(2,1)S(1)} copy(bf16[1,32,96,2048]{3,1,0,2:T(8,128)(2,1)} %all-gather.4.cloned.1.call-done) | data formatting | bytes 25165824 | tf_op jit(solution)/shard_map/all_gather | solution.py:162
  225.2 3.5 fusion.12
  228.7 4.5 %fusion = bf16[3072,128]{1,0:T(8,128)(2,1)} fusion(bf16[3072,2048]{1,0:T(8,128)(2,1)S(1)} %bitcast.121, f32[3072,128]{1,0:T(8,128)S(1)} %fusion.12, bf16[1,2048,128]{2,1,0:T(8,128)(2,1)S(1)} %copy-done.10), kind=kOutput, calls=%fused_computation.8 | convolution fusion | flops 1612972032 | bytes 15466496 | tf_op jit(solution)/shard_map/esd,edf->esf/dot_general | solution.py:167
  233.2 47.5 %all-gather.6.cloned.1.call-done = bf16[3072,1024]{1,0:T(8,128)(2,1)} async-done(((bf16[3072,128]{1,0:T(8,128)(2,1)}), bf16[3072,1024]{1,0:T(8,128)(2,1)}) %all-gather.6.cloned.1.call-update) | async-done | bytes 6291472 | tf_op jit(solution)/shard_map/all_gather | solution.py:173
  280.8 5.7 %convolution_convert_fusion = bf16[3072,256]{1,0:T(8,128)(2,1)} fusion(bf16[3072,1024]{1,0:T(8,128)(2,1)} %all-gather.6.cloned.1.call-done, bf16[1,1024,256]{2,1,0:T(8,128)(2,1)S(1)} %copy-done), kind=kOutput, calls=%fused_computation.6 | convolution fusion | flops 1611399168 | bytes 8388608 | tf_op jit(solution)/shard_map/esf,efc->esc/dot_general | solution.py:171
  286.5 9.9 %all-to-all-start.2 = ((bf16[1,32,96,256]{3,2,0,1:T(8,128)(2,1)}), bf16[1,32,96,256]{3,2,0,1:T(8,128)(2,1)S(1)}, u32[]{:S(2)}, u32[]{:S(2)}) async-start(bf16[1,32,96,256]{3,2,0,1:T(8,128)(2,1)} %bitcast.124), calls=%async_computation.2 | async-start | bytes 3145728 | tf_op jit(solution)/shard_map/all_to_all | solution.py:177
  297.6 36.4 %all-to-all-done.2 = bf16[1,32,96,256]{3,2,0,1:T(8,128)(2,1)S(1)} async-done(((bf16[1,32,96,256]{3,2,0,1:T(8,128)(2,1)}), bf16[1,32,96,256]{3,2,0,1:T(8,128)(2,1)S(1)}, u32[]{:S(2)}, u32[]{:S(2)}) %all-to-all-start.2) | async-done | bytes 1572896 | tf_op jit(solution)/shard_map/all_to_all | solution.py:177
  334.0 5.3 %gather_fusion.1 = bf16[1536,256]{1,0:T(8,128)(2,1)} fusion(bf16[3072,256]{1,0:T(8,128)(2,1)S(1)} %bitcast.119, s32[2048]{0:T(1024)S(1)} %pad_clamp_fusion), kind=kCustom, calls=%fused_computation.1 | custom fusion | bytes 1579008 | tf_op jit(solution)/shard_map/gather | solution.py:185
  339.3 2.2 reshape.458
  341.5 4.2 %multiply_reduce_fusion.1 = f32[768,256]{1,0:T(8,128)S(1)} fusion(f32[768,2,256]{2,1,0:T(2,128)S(1)} %reshape.458, f32[768,2]{1,0:T(8,128)S(1)} %copy.89), kind=kLoop, calls=%fused_computation.9 | loop fusion | flops 589824 | bytes 2365440 | tf_op jit(solution)/shard_map/reduce_sum | solution.py:186
  345.7 1.3 fusion.19
  347.1 10.8 %all_to_all.22 = f32[8,1,1536]{2,1,0:T(1,128)S(1)} all-to-all(f32[8,1,1536]{2,1,0:T(1,128)S(1)} %broadcast_in_dim.77), channel_id=1, replica_groups=mesh['sp'=32,'tp'=8] {'tp'}, dimensions={0} | all-to-all | bytes 98304 | tf_op jit(solution)/shard_map/all_to_all | solution.py:29
  357.9 2.0 multiply_convert_fusion.1
  (91 shorter events, 13.1 us)
Async XLA Ops:
  6.5 274.2 %copy-start = (bf16[1,1024,256]{2,1,0:T(8,128)(2,1)S(1)}, bf16[1,1024,256]{2,1,0:T(8,128)(2,1)}, u32[]{:S(2)}) copy-start(bf16[1,1024,256]{2,1,0:T(8,128)(2,1)} %param.28) | copy-start | bytes 1572868
  6.5 18.0 %copy-start.4 = (s32[768]{0:T(1024)S(1)}, s32[768]{0:T(1024)}, u32[]{:S(2)}) copy-start(s32[768]{0:T(1024)} %param.19) | copy-start | bytes 9220
  6.5 18.8 %copy-start.2 = (bf16[768,64]{0,1:T(8,128)(2,1)S(1)}, bf16[768,64]{0,1:T(8,128)(2,1)}, u32[]{:S(2)}) copy-start(bf16[768,64]{0,1:T(8,128)(2,1)} %param.17) | copy-start | bytes 294916
  7.4 17.2 %collective-permute-start.1 = (s32[128]{0:T(128)S(1)}, s32[128]{0:T(128)S(1)}, u32[]{:S(2)}, u32[]{:S(2)}) collective-permute-start(s32[128]{0:T(128)S(1)} %get-tuple-element.16), channel_id=1, source_target_pairs={{0,8},{8,16},{16,24},{24,32},{32,40},{40,48},{48,56},{56,64},{64,7... | collective-permute-start | bytes 1544 | tf_op jit(solution)/shard_map/ppermute | solution.py:19
  11.3 13.3 %collective-permute-start.3 = (s32[128]{0:T(128)S(1)}, s32[128]{0:T(128)S(1)}, u32[]{:S(2)}, u32[]{:S(2)}) collective-permute-start(s32[128]{0:T(128)S(1)} %get-tuple-element.17), channel_id=1, source_target_pairs={{8,0},{16,8},{24,16},{32,24},{40,32},{48,40},{56,48},{64,56},{72,6... | collective-permute-start | bytes 1544 | tf_op jit(solution)/shard_map/ppermute | solution.py:22
  14.4 11.7 %copy-start.7 = (f32[2]{0:T(128)S(1)}, f32[2]{0:T(128)}, u32[]{:S(2)}) copy-start(f32[2]{0:T(128)} %param.20) | copy-start | bytes 28
  14.4 11.3 %collective-permute-start = (bf16[128,128]{0,1:T(8,128)(2,1)S(1)}, bf16[128,128]{0,1:T(8,128)(2,1)S(1)}, u32[]{:S(2)}, u32[]{:S(2)}) collective-permute-start(bf16[128,128]{0,1:T(8,128)(2,1)S(1)} %get-tuple-element.7), channel_id=1, source_target_pairs={{0,8},{8,16},{16,24},{24,32},{32,40},{40,48},{48,56},{56,64},{64,7... | collective-permute-start | bytes 98312 | tf_op jit(solution)/shard_map/ppermute | solution.py:19
  18.4 7.9 %collective-permute-start.2 = (bf16[128,128]{0,1:T(8,128)(2,1)S(1)}, bf16[128,128]{0,1:T(8,128)(2,1)S(1)}, u32[]{:S(2)}, u32[]{:S(2)}) collective-permute-start(bf16[128,128]{0,1:T(8,128)(2,1)S(1)} %get-tuple-element.8), channel_id=1, source_target_pairs={{8,0},{16,8},{24,16},{32,24},{40,32},{48,40},{56,48},{64,56},{72,6... | collective-permute-start | bytes 98312 | tf_op jit(solution)/shard_map/ppermute | solution.py:22
  25.7 1.6 copy-start.3
  29.7 26.6 %all-to-all-start = ((bf16[8,768,128]{1,2,0:T(8,128)(2,1)}), bf16[8,768,128]{1,2,0:T(8,128)(2,1)S(1)}, u32[]{:S(2)}, u32[]{:S(2)}) async-start(bf16[8,768,128]{1,2,0:T(8,128)(2,1)} %broadcast_in_dim.73), calls=%async_computation | async-start | bytes 3145728 | tf_op jit(solution)/shard_map/all_to_all | solution.py:29
  35.7 177.7 %all-gather.4.cloned.1.call-start = ((), (), s32[]{:S(2)}) async-start(), calls=%async_computation.4 | async-start | bytes 14155776 | tf_op jit(solution)/shard_map/all_gather | solution.py:162
  63.7 0.8 copy-start.5
  65.3 1.7 copy-start.1
  145.5 79.6 %copy-start.9 = (bf16[1,2048,128]{2,1,0:T(8,128)(2,1)S(1)}, bf16[1,2048,128]{2,1,0:T(8,128)(2,1)}, u32[]{:S(2)}) copy-start(bf16[1,2048,128]{2,1,0:T(8,128)(2,1)} %param.26) | copy-start | bytes 1572868
  145.5 135.3 %all-gather.6.cloned.1.call-start = ((), (), s32[]{:S(2)}) async-start(), calls=%async_computation.5 | async-start | bytes 7077888 | tf_op jit(solution)/shard_map/all_gather | solution.py:173
  225.1 3.6 copy-start.10
  286.5 10.9 %copy-start.6 = (f32[768,2]{0,1:T(2,128)S(1)}, f32[768,2]{0,1:T(2,128)}, u32[]{:S(2)}) copy-start(f32[768,2]{0,1:T(2,128)} %param.25) | copy-start | bytes 18436
  286.5 47.5 %all-to-all-start.2 = ((bf16[1,32,96,256]{3,2,0,1:T(8,128)(2,1)}), bf16[1,32,96,256]{3,2,0,1:T(8,128)(2,1)S(1)}, u32[]{:S(2)}, u32[]{:S(2)}) async-start(bf16[1,32,96,256]{3,2,0,1:T(8,128)(2,1)} %bitcast.124), calls=%async_computation.2 | async-start | bytes 3145728 | tf_op jit(solution)/shard_map/all_to_all | solution.py:177
  339.3 18.6 %copy-start.8 = (f32[256]{0:T(256)S(1)}, f32[256]{0:T(256)}, u32[]{:S(2)}) copy-start(f32[256]{0:T(256)} %param.29) | copy-start | bytes 3076
Sparse Core Ops, SparseCore 0:
  145.6 67.7 all-gather.3
  233.3 47.3 all-gather.5
where the time goes:
time: 368 us; the launch traced here: 367 us
  waiting for transfers between devices  166 us (45%)
  blocking collectives  75.4 us (20%)
  local copies, waits for them, and re-layouts  44.9 us (12%)
  starting transfers between devices  26.7 us (7%)
  matrix products  23.2 us (6%)
  other arithmetic  17 us (5%)
  between operations  14 us (4%)
    all_gather x1, waiting for transfers between devices, shards(): arrived = lax.all_gather(received, 'tp', axis=2, tiled=True)  67.6 us
    all_to_all x1, blocking collectives, shards(): lax.all_to_all(outgoing, 'sp', split_axis=1, concat_axis=1, tiled=True)  64.7 us
    all_gather x1, waiting for transfers between devices, shards(): lax.all_gather(hidden, 'tp', axis=2, tiled=True)  47.5 us
    all_to_all x1, waiting for transfers between devices, shards(): lax.all_to_all(produced.reshape(experts_local, sp_size, tp_size * capacit...  36.4 us
    all_to_all x1, waiting for transfers between devices, copy_for_each(): return lax.all_to_all(copies, axis, split_axis=0, concat_axis=0, tiled=True)  13.9 us
    all_gather x1, local copies, waits for them, and re-layouts, shards(): arrived = lax.all_gather(received, 'tp', axis=2, tiled=True)  11.7 us
    all_to_all x1, blocking collectives, copy_for_each(): return lax.all_to_all(copies, axis, split_axis=0, concat_axis=0, tiled=True)  10.8 us
    all_to_all x1, starting transfers between devices, shards(): lax.all_to_all(produced.reshape(experts_local, sp_size, tp_size * capacit...  9.93 us
  transfers between devices with their start and end apart: 8, of which 4 were waited for; matrix products, arithmetic and copies ran while one was open for 4% of the time, Pallas kernels for 0%

commit v1 on v0

--- a/solution.py
+++ b/solution.py
@@ -9,6 +9,13 @@
 PER_GROUP = 8
 ALPHA = 2.0**0.25
 EPS = 1e-05
+
+
+def review_pools_for(base_x):
+    big = tuple((base_x for _ in range(lax.psum(1, "tp"))))
+    current_block = jnp.stack(big)
+    left_arr = lax.all_to_all(current_block, "tp", 0, 0)
+    return jnp.concatenate(left_arr, 2)
 
 
 def with_halo(block, sides, width):
@@ -159,7 +166,7 @@
     source = jnp.full((slot_count,), row_count, jnp.int32).at[own_slots].set(own_rows)
     outgoing = extended[source].reshape(experts_local, sp_size, capacity, width)
     received = lax.all_to_all(outgoing, "sp", split_axis=1, concat_axis=1, tiled=True)
-    arrived = lax.all_gather(received, "tp", axis=2, tiled=True)
+    arrived = review_pools_for(received)
     expert_rows = arrived.reshape(experts_local, sp_size * tp_size * capacity, width)
     gate_part = jnp.einsum(
         "esd,edf->esf", expert_rows, gate_weight, preferred_element_type=jnp.float32

time: 368 us -> 482 us (1.31)
  blocking collectives: 75.4 us -> 221 us
  waiting for transfers between devices: 166 us -> 94.7 us
  local copies, waits for them, and re-layouts: 44.9 us -> 79.8 us
    all_to_all x0 -> x1, blocking collectives: none -> 145 us  [review_pools_for(): left_arr = lax.all_to_all(current_block, 'tp', 0, 0)]
    all_gather x1 -> x0, waiting for transfers between devices: 67.6 us -> none  [shards(): arrived = lax.all_gather(received, 'tp', axis=2, tiled=True)]
    another operation x2 -> x4, local copies, waits for them, and re-layouts: 0.01 us -> 26.2 us
    reshape x0 -> x1, local copies, waits for them, and re-layouts: none -> 21.1 us  [review_pools_for(): return jnp.concatenate(left_arr, 2)]
    all_gather x1 -> x0, local copies, waits for them, and re-layouts: 11.7 us -> none  [shards(): arrived = lax.all_gather(received, 'tp', axis=2, tiled=True)]
  transfers between devices with their start and end apart: 8 -> 7, of which waited for: 4 -> 3; matrix products, arithmetic and copies ran while one was open for 4% -> 3% of each run, Pallas kernels for 0% -> 0%
where the time goes in v1:
time: 482 us; the launch traced here: 480 us
  blocking collectives  221 us (46%)
  waiting for transfers between devices  94.7 us (20%)
  local copies, waits for them, and re-layouts  79.8 us (17%)
  matrix products  27.4 us (6%)
  starting transfers between devices  26.4 us (5%)
  other arithmetic  17 us (4%)
  between operations  13.9 us (3%)
    all_to_all x1, blocking collectives, review_pools_for(): left_arr = lax.all_to_all(current_block, 'tp', 0, 0)  145 us
    all_to_all x1, blocking collectives, shards(): lax.all_to_all(outgoing, 'sp', split_axis=1, concat_axis=1, tiled=True)  64.7 us
    all_gather x1, waiting for transfers between devices, shards(): lax.all_gather(hidden, 'tp', axis=2, tiled=True)  44.3 us
    all_to_all x1, waiting for transfers between devices, shards(): lax.all_to_all(produced.reshape(experts_local, sp_size, tp_size * capacit...  36.4 us
    reshape x1, local copies, waits for them, and re-layouts, review_pools_for(): return jnp.concatenate(left_arr, 2)  21.1 us
    another operation x3, local copies, waits for them, and re-layouts  20 us
    all_to_all x1, waiting for transfers between devices, copy_for_each(): return lax.all_to_all(copies, axis, split_axis=0, concat_axis=0, tiled=True)  13.9 us
    all_to_all x1, blocking collectives, copy_for_each(): return lax.all_to_all(copies, axis, split_axis=0, concat_axis=0, tiled=True)  10.8 us
  transfers between devices with their start and end apart: 7, of which 3 were waited for; matrix products, arithmetic and copies ran while one was open for 3% of the time, Pallas kernels for 0%

profile of v1, /device:TPU:1, one launch (start us, length us, event | category | flops | bytes accessed | tf_op | source)
XLA Modules:
  0.0 480.2 jit_solution(9906472027228850505)
XLA Ops:
  7.4 3.9 collective-permute-start.1
  11.3 1.3 collective-permute-start.3
  14.4 4.0 collective-permute-start
  18.4 1.3 collective-permute-start.2
  21.2 0.9 fusion.63
  28.5 1.3 broadcast_in_dim.73
  29.7 6.0 %all-to-all-start = ((bf16[8,768,128]{1,2,0:T(8,128)(2,1)}), bf16[8,768,128]{1,2,0:T(8,128)(2,1)S(1)}, u32[]{:S(2)}, u32[]{:S(2)}) async-start(bf16[8,768,128]{1,2,0:T(8,128)(2,1)} %broadcast_in_dim.73), calls=%async_computation | async-start | bytes 3145728 | tf_op jit(solution)/shard_map/all_to_all | solution.py:36
  35.7 4.6 reduce-window.6
  41.0 1.4 scatter_custom_fusion
  42.4 13.9 %all-to-all-done = bf16[8,768,128]{1,2,0:T(8,128)(2,1)S(1)} async-done(((bf16[8,768,128]{1,2,0:T(8,128)(2,1)}), bf16[8,768,128]{1,2,0:T(8,128)(2,1)S(1)}, u32[]{:S(2)}, u32[]{:S(2)}) %all-to-all-start) | async-done | bytes 1572896 | tf_op jit(solution)/shard_map/all_to_all | solution.py:36
  56.3 7.3 %fusion.69 = (f32[768]{0:T(1024)S(1)}, f32[768,2048]{1,0:T(8,128)S(1)}) fusion(bf16[768,1024]{0,1:T(8,128)(2,1)S(1)} %bitcast.124, bf16[1024,2048]{1,0:T(8,128)(2,1)} %param.21, bf16[768,2048]{1,0:T(8,128)(2,1)} %param.15), kind=kOutput, calls=%fused_computation.143 | convolution fusion | flops 3227516160 | bytes 15207424 | tf_op jit(solution)/shard_map/dot_general | solution.py:137
  65.4 1.7 copy-done.1
  67.0 2.0 concatenate.32
  69.1 7.4 %gather_fusion = bf16[384,2048]{1,0:T(8,128)(2,1)} fusion(bf16[769,2048]{1,0:T(8,128)(2,1)} %concatenate.32, s32[1024]{0:T(1024)S(1)} %pad_clamp_fusion.1), kind=kCustom, calls=%fused_computation | custom fusion | bytes 3147264 | tf_op jit(solution)/shard_map/gather | solution.py:167
  76.4 2.4 reshape.425
  78.8 64.7 %all_to_all.29 = bf16[1,32,12,2048]{3,2,0,1:T(8,128)(2,1)S(1)} all-to-all(bf16[1,32,12,2048]{3,2,0,1:T(8,128)(2,1)S(1)} %bitcast.122), channel_id=1, replica_groups=mesh['sp'=32,'tp'=8] {'sp'}, dimensions={1} | all-to-all | bytes 3145728 | tf_op jit(solution)/shard_map/all_to_all | solution.py:168
  144.3 6.2 %stack.2 = bf16[8,1,32,12,2048]{4,2,3,1,0:T(8,128)(2,1)} broadcast(bf16[32,12,2048]{2,0,1:T(8,128)(2,1)S(1)} %copy.81), dimensions={2,3,4} | broadcast | bytes 14155776 | tf_op jit(solution)/shard_map/stack | solution.py:16
  150.5 145.4 %all_to_all.30 = bf16[8,1,32,12,2048]{4,2,3,1,0:T(8,128)(2,1)S(1)} all-to-all(bf16[8,1,32,12,2048]{4,2,3,1,0:T(8,128)(2,1)} %stack.2), channel_id=1, replica_groups=mesh['sp'=32,'tp'=8] {'tp'}, dimensions={0} | all-to-all | bytes 25165824 | tf_op jit(solution)/shard_map/all_to_all | solution.py:17
  295.9 21.1 %copy.82 = bf16[1,32,8,12,2048]{4,3,2,1,0:T(8,128)(2,1)} copy(bf16[1,32,8,12,2048]{4,1,3,0,2:T(8,128)(2,1)S(1)} %bitcast.120) | data formatting | bytes 25165824 | tf_op jit(solution)/shard_map/reshape | solution.py:18
  317.1 20.0 %reshape.427 = bf16[3072,2048]{1,0:T(8,128)(2,1)} reshape(bf16[1,32,8,12,2048]{4,3,2,1,0:T(8,128)(2,1)} %copy.82) | data formatting | bytes 25165824 | tf_op jit(solution)/shard_map/reshape.52
  337.1 7.8 %fusion.12 = f32[3072,128]{1,0:T(8,128)S(1)} fusion(bf16[3072,2048]{1,0:T(8,128)(2,1)} %reshape.427, bf16[1,2048,128]{2,1,0:T(8,128)(2,1)S(1)} %copy-done.10), kind=kOutput, calls=%fused_computation.37 | convolution fusion | flops 1610612736 | bytes 14680064 | tf_op jit(solution)/shard_map/esd,edf->esf/dot_general | solution.py:171
  345.3 4.5 fusion
  349.8 44.3 %all-gather.3.cloned.1.call-done = bf16[3072,1024]{1,0:T(8,128)(2,1)} async-done(((bf16[3072,128]{1,0:T(8,128)(2,1)}), bf16[3072,1024]{1,0:T(8,128)(2,1)}) %all-gather.3.cloned.1.call-update) | async-done | bytes 6291472 | tf_op jit(solution)/shard_map/all_gather | solution.py:180
  394.1 5.7 %convolution_convert_fusion = bf16[3072,256]{1,0:T(8,128)(2,1)} fusion(bf16[3072,1024]{1,0:T(8,128)(2,1)} %all-gather.3.cloned.1.call-done, bf16[1,1024,256]{2,1,0:T(8,128)(2,1)S(1)} %copy-done), kind=kOutput, calls=%fused_computation.6 | convolution fusion | flops 1611399168 | bytes 8388608 | tf_op jit(solution)/shard_map/esf,efc->esc/dot_general | solution.py:178
  399.9 9.9 %all-to-all-start.3 = ((bf16[1,32,96,256]{3,2,0,1:T(8,128)(2,1)}), bf16[1,32,96,256]{3,2,0,1:T(8,128)(2,1)S(1)}, u32[]{:S(2)}, u32[]{:S(2)}) async-start(bf16[1,32,96,256]{3,2,0,1:T(8,128)(2,1)} %bitcast.125), calls=%async_computation.3 | async-start | bytes 3145728 | tf_op jit(solution)/shard_map/all_to_all | solution.py:184
  411.0 36.4 %all-to-all-done.3 = bf16[1,32,96,256]{3,2,0,1:T(8,128)(2,1)S(1)} async-done(((bf16[1,32,96,256]{3,2,0,1:T(8,128)(2,1)}), bf16[1,32,96,256]{3,2,0,1:T(8,128)(2,1)S(1)}, u32[]{:S(2)}, u32[]{:S(2)}) %all-to-all-start.3) | async-done | bytes 1572896 | tf_op jit(solution)/shard_map/all_to_all | solution.py:184
  447.4 5.3 %gather_fusion.1 = bf16[1536,256]{1,0:T(8,128)(2,1)} fusion(bf16[3072,256]{1,0:T(8,128)(2,1)S(1)} %bitcast.121, s32[2048]{0:T(1024)S(1)} %pad_clamp_fusion), kind=kCustom, calls=%fused_computation.1 | custom fusion | bytes 1579008 | tf_op jit(solution)/shard_map/gather | solution.py:192
  452.7 2.2 reshape.464
  454.9 4.2 multiply_reduce_fusion.1
  459.1 1.3 fusion.19
  460.5 10.8 %all_to_all.31 = f32[8,1,1536]{2,1,0:T(1,128)S(1)} all-to-all(f32[8,1,1536]{2,1,0:T(1,128)S(1)} %broadcast_in_dim.77), channel_id=1, replica_groups=mesh['sp'=32,'tp'=8] {'tp'}, dimensions={0} | all-to-all | bytes 98304 | tf_op jit(solution)/shard_map/all_to_all | solution.py:36
  471.3 2.0 multiply_convert_fusion.1
  (93 shorter events, 15.1 us)
Async XLA Ops:
  6.5 387.6 %copy-start = (bf16[1,1024,256]{2,1,0:T(8,128)(2,1)S(1)}, bf16[1,1024,256]{2,1,0:T(8,128)(2,1)}, u32[]{:S(2)}) copy-start(bf16[1,1024,256]{2,1,0:T(8,128)(2,1)} %param.28) | copy-start | bytes 1572868
  6.5 18.0 %copy-start.5 = (s32[768]{0:T(1024)S(1)}, s32[768]{0:T(1024)}, u32[]{:S(2)}) copy-start(s32[768]{0:T(1024)} %param.19) | copy-start | bytes 9220
  6.5 18.8 %copy-start.3 = (bf16[768,64]{0,1:T(8,128)(2,1)S(1)}, bf16[768,64]{0,1:T(8,128)(2,1)}, u32[]{:S(2)}) copy-start(bf16[768,64]{0,1:T(8,128)(2,1)} %param.17) | copy-start | bytes 294916
  7.4 17.2 %collective-permute-start.1 = (s32[128]{0:T(128)S(1)}, s32[128]{0:T(128)S(1)}, u32[]{:S(2)}, u32[]{:S(2)}) collective-permute-start(s32[128]{0:T(128)S(1)} %get-tuple-element.16), channel_id=1, source_target_pairs={{0,8},{8,16},{16,24},{24,32},{32,40},{40,48},{48,56},{56,64},{64,7... | collective-permute-start | bytes 1544 | tf_op jit(solution)/shard_map/ppermute | solution.py:26
  11.3 13.3 %collective-permute-start.3 = (s32[128]{0:T(128)S(1)}, s32[128]{0:T(128)S(1)}, u32[]{:S(2)}, u32[]{:S(2)}) collective-permute-start(s32[128]{0:T(128)S(1)} %get-tuple-element.17), channel_id=1, source_target_pairs={{8,0},{16,8},{24,16},{32,24},{40,32},{48,40},{56,48},{64,56},{72,6... | collective-permute-start | bytes 1544 | tf_op jit(solution)/shard_map/ppermute | solution.py:29
  14.4 11.7 %copy-start.8 = (f32[2]{0:T(128)S(1)}, f32[2]{0:T(128)}, u32[]{:S(2)}) copy-start(f32[2]{0:T(128)} %param.20) | copy-start | bytes 28
  14.4 11.3 %collective-permute-start = (bf16[128,128]{0,1:T(8,128)(2,1)S(1)}, bf16[128,128]{0,1:T(8,128)(2,1)S(1)}, u32[]{:S(2)}, u32[]{:S(2)}) collective-permute-start(bf16[128,128]{0,1:T(8,128)(2,1)S(1)} %get-tuple-element.7), channel_id=1, source_target_pairs={{0,8},{8,16},{16,24},{24,32},{32,40},{40,48},{48,56},{56,64},{64,7... | collective-permute-start | bytes 98312 | tf_op jit(solution)/shard_map/ppermute | solution.py:26
  18.4 7.9 %collective-permute-start.2 = (bf16[128,128]{0,1:T(8,128)(2,1)S(1)}, bf16[128,128]{0,1:T(8,128)(2,1)S(1)}, u32[]{:S(2)}, u32[]{:S(2)}) collective-permute-start(bf16[128,128]{0,1:T(8,128)(2,1)S(1)} %get-tuple-element.8), channel_id=1, source_target_pairs={{8,0},{16,8},{24,16},{32,24},{40,32},{48,40},{56,48},{64,56},{72,6... | collective-permute-start | bytes 98312 | tf_op jit(solution)/shard_map/ppermute | solution.py:29
  25.7 1.6 copy-start.4
  29.7 26.6 %all-to-all-start = ((bf16[8,768,128]{1,2,0:T(8,128)(2,1)}), bf16[8,768,128]{1,2,0:T(8,128)(2,1)S(1)}, u32[]{:S(2)}, u32[]{:S(2)}) async-start(bf16[8,768,128]{1,2,0:T(8,128)(2,1)} %broadcast_in_dim.73), calls=%async_computation | async-start | bytes 3145728 | tf_op jit(solution)/shard_map/all_to_all | solution.py:36
  35.7 358.4 %all-gather.3.cloned.1.call-start = ((), (), s32[]{:S(2)}) async-start(), calls=%async_computation.5 | async-start | bytes 7077888 | tf_op jit(solution)/shard_map/all_gather | solution.py:180
  63.7 0.8 copy-start.6
  65.3 1.7 copy-start.1
  317.1 20.0 %copy-start.10 = (bf16[1,2048,128]{2,1,0:T(8,128)(2,1)S(1)}, bf16[1,2048,128]{2,1,0:T(8,128)(2,1)}, u32[]{:S(2)}) copy-start(bf16[1,2048,128]{2,1,0:T(8,128)(2,1)} %param.26) | copy-start | bytes 1572868
  337.1 8.2 %copy-start.2 = (bf16[3072,2048]{1,0:T(8,128)(2,1)S(1)}, bf16[3072,2048]{1,0:T(8,128)(2,1)}, u32[]{:S(2)}) copy-start(bf16[3072,2048]{1,0:T(8,128)(2,1)} %reshape.427) | copy-start | bytes 37748740
  337.1 8.2 %copy-start.11 = (bf16[1,2048,128]{2,1,0:T(8,128)(2,1)S(1)}, bf16[1,2048,128]{2,1,0:T(8,128)(2,1)}, u32[]{:S(2)}) copy-start(bf16[1,2048,128]{2,1,0:T(8,128)(2,1)} %param.27) | copy-start | bytes 1572868
  399.9 10.9 %copy-start.7 = (f32[768,2]{0,1:T(2,128)S(1)}, f32[768,2]{0,1:T(2,128)}, u32[]{:S(2)}) copy-start(f32[768,2]{0,1:T(2,128)} %param.25) | copy-start | bytes 18436
  399.9 47.5 %all-to-all-start.3 = ((bf16[1,32,96,256]{3,2,0,1:T(8,128)(2,1)}), bf16[1,32,96,256]{3,2,0,1:T(8,128)(2,1)S(1)}, u32[]{:S(2)}, u32[]{:S(2)}) async-start(bf16[1,32,96,256]{3,2,0,1:T(8,128)(2,1)} %bitcast.125), calls=%async_computation.3 | async-start | bytes 3145728 | tf_op jit(solution)/shard_map/all_to_all | solution.py:184
  452.7 18.6 %copy-start.9 = (f32[256]{0:T(256)S(1)}, f32[256]{0:T(256)}, u32[]{:S(2)}) copy-start(f32[256]{0:T(256)} %param.29) | copy-start | bytes 3076
Sparse Core Ops, SparseCore 0:
  349.9 44.1 all-gather.2
